TPU v7x, 32 devices: a whole 2x2x4 slice. The times are simulated.
32 devices in a mesh: grp: 2 (over y), sp: 4 (over z), tp: 4 (over x, core).
Axes of the slice: x: 2, y: 2, z: 4, core: 2. Of those that a mesh axis runs over, the one named last changes fastest.
Arguments:
- queries: bfloat16 [2048, 2048], P(('grp', 'sp'), 'tp'), parts along dimension 0, may hold values from -6 to 6
- keys: bfloat16 [2048, 512], P(('grp', 'sp'), 'tp'), parts along dimension 0, may hold values from -6 to 6
- values: bfloat16 [2048, 512], P(('grp', 'sp'), 'tp'), parts along dimension 0, may hold values from -6 to 6
- query_gain: float32 [128], replicated, may hold values from 1 to 5, as said below
- key_norm_gain: float32 [128], replicated, may hold values from 1 to 5, as said below
- out_weight: bfloat16 [2048, 2048], P('tp'), may hold values from -0.125 to 0.125
- residual: bfloat16 [2048, 2048], P(('grp', 'sp')), parts along dimension 0, may hold values from -0.59765625 to 0.59765625
- mixer_gain: float32 [2048], replicated, may hold values from 0.1 to 1.9
- gate_weight: bfloat16 [2048, 5632], P('sp', 'tp'), may hold values from -0.125 to 0.125
- up_weight: bfloat16 [2048, 5632], P('sp', 'tp'), may hold values from -0.125 to 0.125
- conv_taps: float32 [3, 5632], P(None, 'tp'), may hold values from -3.5 to 3.5
- down_weight: bfloat16 [5632, 2048], P('tp', 'sp'), may hold values from -0.078125 to 0.078125
Outputs:
- layer_out: bfloat16 [2048, 2048], P(('grp', 'sp', 'tp')), parts along dimension 0
There are 2 independent parts, one for each index of `grp`. A program takes and returns all parts, laid end to end along the dimension named above; an argument that names none is the same for every part. Nothing has to cross between parts.
Inputs may be any that keep to these rules, and one draw needn't show every extreme that they name: `query_gain`: positive. `key_norm_gain`: positive.
All inputs are finite; a program needn't handle non-finite values.
Results may differ from a plain program's by a relative error of at most 0.024.
Values may be sent and summed in bfloat16 or wider, within the bound.
A program may use at most 128 MiB of HBM per device.

v0:
```python
import math

import jax
import jax.numpy as jnp
from jax import lax
from jax.sharding import PartitionSpec as P

GRID = 64


norm_eps = 1e-06
rope_base = 10000.0


def padded_2(block, sides, width):
    for axis, dim in sides:
        count = lax.axis_size(axis)
        forward = [(i, i + 1) for i in range(count - 1)]
        backward = [(target, source) for source, target in forward]
        low = lax.ppermute(
            lax.slice_in_dim(block, block.shape[dim] - width, None, axis=dim), axis, forward
        )
        high = lax.ppermute(lax.slice_in_dim(block, 0, width, axis=dim), axis, backward)
        block = jnp.concatenate([low, block, high], axis=dim)
    return block


def angle_tables(positions, head_dim):
    quarter = head_dim // 4
    freqs = 1.0 / rope_base ** (jnp.arange(quarter, dtype=jnp.float32) * 4.0 / head_dim)
    grid_row = (positions // GRID).astype(jnp.float32)
    grid_col = (positions % GRID).astype(jnp.float32)
    by_row = grid_row[:, None] * freqs[None, :]
    by_col = grid_col[:, None] * freqs[None, :]
    angles = jnp.concatenate([by_row, by_row, by_col, by_col], axis=-1)
    return (jnp.cos(angles), jnp.sin(angles))


def apply_rotary(field, cosine_table, sine_table):
    half = field.shape[-1] // 2
    quarter = half // 2
    first = field[..., :half]
    second = field[..., half:]
    turned = jnp.concatenate(
        [
            -first[..., quarter:],
            first[..., :quarter],
            -second[..., quarter:],
            second[..., :quarter],
        ],
        axis=-1,
    )
    return field * cosine_table[:, None, :] + turned * sine_table[:, None, :]


def per_head_norm(field, gain):
    floats = field.astype(jnp.float32)
    return floats * lax.rsqrt(jnp.mean(floats * floats, axis=-1, keepdims=True) + norm_eps) * gain


def local(
    queries,
    keys,
    values,
    query_gain,
    key_norm_gain,
    out_weight,
    residual,
    mixer_gain,
    gate_weight,
    up_weight,
    conv_taps,
    down_weight,
):
    tok_rows = queries.shape[0]
    head_dim = query_gain.shape[0]
    heads_here = queries.shape[1] // head_dim
    kv_here = keys.shape[1] // head_dim
    query_group = heads_here // kv_here
    part_rows = tok_rows // lax.axis_size("tp")
    positions = lax.axis_index("sp") * tok_rows + jnp.arange(tok_rows, dtype=jnp.int32)
    cosine_table, sine_table = angle_tables(positions, head_dim)
    rotated_queries = apply_rotary(
        per_head_norm(queries.reshape(tok_rows, heads_here, head_dim), query_gain),
        cosine_table,
        sine_table,
    ).astype(jnp.bfloat16)
    rotated_keys = apply_rotary(
        per_head_norm(keys.reshape(tok_rows, kv_here, head_dim), key_norm_gain),
        cosine_table,
        sine_table,
    ).astype(jnp.bfloat16)
    key_flat = rotated_keys.reshape(tok_rows, kv_here * head_dim)
    query_mat = jnp.transpose(
        rotated_queries.reshape(tok_rows, kv_here, query_group, head_dim), (1, 2, 0, 3)
    )
    query_mat = query_mat.reshape(kv_here, query_group * tok_rows, head_dim)
    scale = head_dim ** (-0.5)
    start_state = (
        jnp.full((kv_here, query_group * tok_rows), -jnp.inf, jnp.float32),
        jnp.zeros((kv_here, query_group * tok_rows), jnp.float32),
        jnp.zeros((kv_here, query_group * tok_rows, head_dim), jnp.float32),
    )
    key_piece = lax.all_gather(key_flat, "sp", axis=0, tiled=True)
    value_piece = lax.all_gather(values, "sp", axis=0, tiled=True)
    piece_rows = key_piece.shape[0]
    block_slice = math.gcd(piece_rows, 512)
    key_blocks = key_piece.reshape(piece_rows // block_slice, block_slice, kv_here, head_dim)
    value_blocks = value_piece.reshape(piece_rows // block_slice, block_slice, kv_here, head_dim)

    def one_block(state, block_pair):
        running, totals, accum = state
        key_block, value_block = block_pair
        scores = (
            jnp.einsum("hqd,khd->hqk", query_mat, key_block, preferred_element_type=jnp.float32)
            * scale
        )
        new_max = jnp.maximum(running, jnp.max(scores, axis=-1))
        factor = jnp.exp(running - new_max)
        expo = jnp.exp(scores - new_max[..., None])
        totals = totals * factor + jnp.sum(expo, axis=-1)
        accum = accum * factor[..., None] + jnp.einsum(
            "hqk,khd->hqd",
            expo.astype(jnp.bfloat16),
            value_block,
            preferred_element_type=jnp.float32,
        )
        return ((new_max, totals, accum), None)

    result, unused = lax.scan(one_block, start_state, (key_blocks, value_blocks))
    running, totals, accum = result
    heads = (accum / totals[..., None]).astype(jnp.bfloat16)
    heads = jnp.transpose(heads.reshape(kv_here, query_group, tok_rows, head_dim), (2, 0, 1, 3))
    heads = heads.reshape(tok_rows, heads_here * head_dim)
    own_start = lax.axis_index("tp") * part_rows
    full_proj = lax.psum(
        jnp.dot(heads, out_weight, preferred_element_type=jnp.float32).astype(jnp.bfloat16), "tp"
    ).astype(jnp.float32)
    mixed = residual.astype(jnp.float32) + full_proj
    normed = per_head_norm(mixed, mixer_gain).astype(jnp.bfloat16)
    mixed_keep = lax.dynamic_slice_in_dim(mixed, own_start, part_rows, 0)
    gate_acc = jnp.dot(
        normed,
        lax.all_gather(gate_weight, "sp", axis=0, tiled=True),
        preferred_element_type=jnp.float32,
    )
    up_acc = jnp.dot(
        normed,
        lax.all_gather(up_weight, "sp", axis=0, tiled=True),
        preferred_element_type=jnp.float32,
    )
    gate = gate_acc.astype(jnp.bfloat16)
    up_val = up_acc.astype(jnp.bfloat16)
    padded = padded_2(gate, (("sp", 0),), 1).astype(jnp.float32)
    conv = conv_taps[0] * padded[:-2] + conv_taps[1] * padded[1:-1] + conv_taps[2] * padded[2:]
    hidden = (jax.nn.silu(conv) * up_val.astype(jnp.float32)).astype(jnp.bfloat16)
    down_full = lax.all_gather(down_weight, "sp", axis=1, tiled=True)
    mixer_out = lax.psum_scatter(
        jnp.dot(hidden, down_full, preferred_element_type=jnp.float32).astype(jnp.bfloat16),
        "tp",
        scatter_dimension=0,
        tiled=True,
    ).astype(jnp.float32)
    return (mixed_keep + mixer_out).astype(jnp.bfloat16)


def solution(mesh):
    in_specs = (
        P(("grp", "sp"), "tp"),
        P(("grp", "sp"), "tp"),
        P(("grp", "sp"), "tp"),
        P(),
        P(),
        P("tp", None),
        P(("grp", "sp"), None),
        P(),
        P("sp", "tp"),
        P("sp", "tp"),
        P(None, "tp"),
        P("tp", "sp"),
    )
    out_specs = P(("grp", "sp", "tp"), None)
    return jax.shard_map(local, mesh=mesh, in_specs=in_specs, out_specs=out_specs, check_vma=False)
```

profile of v0, /device:TPU:0, one launch (start us, length us, event | category | flops | bytes accessed | tf_op | source)
XLA Modules:
  0.0 424.0 jit_solution(16997622798966750573)
XLA Ops:
  7.4 0.0 copy-start
  7.4 0.0 all-reduce.2.cloned.1.call-start
  7.4 1.3 reshape.324
  8.7 1.9 reshape.323
  10.6 1.0 fusion.32
  11.5 0.9 fusion.34
  12.5 0.2 fusion.39
  12.7 0.3 multiply_reduce_fusion.2
  13.0 0.0 copy-done.7
  13.1 0.3 multiply_multiply_fusion
  13.4 0.0 copy-start.3
  13.4 0.0 copy-start.6
  13.4 0.0 copy-start.2
  13.4 0.9 fusion.28
  14.3 0.1 broadcast_multiply_fusion.1
  14.5 0.0 copy-done.3
  14.5 0.0 copy-done.6
  14.5 0.6 fusion.37
  15.1 0.0 copy-start.4
  15.1 0.0 copy-done.2
  15.2 1.2 fusion.31
  16.4 15.7 %all_gather.15 = bf16[1024,128]{1,0:T(8,128)(2,1)S(1)} all-gather(bf16[256,128]{1,0:T(8,128)(2,1)S(1)} %get-tuple-element.109), channel_id=1, replica_groups=mesh['grp'=2,'sp'=4,'tp'=4] {'sp'}, dimensions={0}, use_global_device_ids=true | all-gather | bytes 327680 | tf_op jit(solution)/shard_map/all_gather | solution.py:104
  32.0 0.0 copy-done.4
  32.0 14.6 %all_gather.16 = bf16[1024,128]{1,0:T(8,128)(2,1)S(1)} all-gather(bf16[256,128]{1,0:T(8,128)(2,1)S(1)} %copy-done.4), channel_id=1, replica_groups=mesh['grp'=2,'sp'=4,'tp'=4] {'sp'}, dimensions={0}, use_global_device_ids=true | all-gather | bytes 327680 | tf_op jit(solution)/shard_map/all_gather | solution.py:105
  46.6 9.3 %while.15 = (s32[]{:T(128)}, f32[1,1024]{1,0:T(1,128)S(1)}, f32[1,1024]{1,0:T(1,128)S(1)}, f32[1,1024,128]{2,1,0:T(8,128)S(1)}, bf16[2,512,1,128]{3,1,2,0:T(8,12...) while((s32[]{:T(128)}, f32[1,1024]{1,0:T(1,128)S(1)}, ...), condition=%wide.region_5.6_spmd.clone, body=%wide.region_2.5_spmd.clone.sunk | while | flops 273028096 | bytes 16318605 | solution.py:130
  46.6 1.8 multiply_reduce_fusion.4
  48.4 2.1 fusion.63
  50.5 0.1 copy-done.1
  50.6 0.6 fusion.65
  51.3 1.8 multiply_reduce_fusion.4
  53.1 2.1 fusion.63
  55.2 0.1 copy-done.1
  55.3 0.6 fusion.65
  55.9 0.2 divide_convert_fusion
  56.1 0.1 copy.27
  56.3 0.0 copy-done
  56.3 1.7 convolution_convert_fusion
  58.0 0.0 all-reduce.2.cloned.1.call-update
  58.0 0.0 all-gather.4.cloned.1.call-start
  58.1 0.5 all-gather.4.cloned.1.call-update
  58.6 0.0 all-gather.6.cloned.1.call-start
  58.7 0.5 all-gather.6.cloned.1.call-update
  59.2 0.0 all-gather.8.cloned.1.call-start
  59.2 0.5 all-gather.8.cloned.1.call-update
  59.8 0.0 copy-start.8
  59.8 0.0 reduce-scatter.2.cloned.1.call-start
  59.8 35.8 %all-reduce.2.cloned.1.call-done = bf16[256,2048]{1,0:T(8,128)(2,1)} async-done(((bf16[256,2048]{1,0:T(8,128)(2,1)}), bf16[256,2048]{1,0:T(8,128)(2,1)}) %all-reduce.2.cloned.1.call-update) | async-done | bytes 1048592 | tf_op jit(solution)/shard_map/psum | solution.py:136
  95.7 3.2 convert_add_fusion
  98.9 68.7 %all-gather.4.cloned.1.call-done = bf16[2048,1408]{1,0:T(8,128)(2,1)} async-done(((bf16[512,1408]{1,0:T(8,128)(2,1)}), bf16[2048,1408]{1,0:T(8,128)(2,1)}) %all-gather.4.cloned.1.call-update) | async-done | bytes 5767184 | tf_op jit(solution)/shard_map/all_gather | solution.py:144
  167.6 0.0 copy-done.8
  167.6 5.1 %convolution_convert_fusion.2 = bf16[256,1408]{1,0:T(8,128)(2,1)S(1)} fusion(bf16[2048,1408]{1,0:T(8,128)(2,1)} %all-gather.4.cloned.1.call-done, f32[2048]{0:T(1024)S(1)} %copy-done.8, f32[256]{0:T(256)S(1)} %add_rsqrt_fusion.1, bf16[256,2048]{1,0:T(8,128)(2,1)} %all-reduce.2.cloned.1.call-done, bf16[256,2048]{1,0:T(8,128)(2,1)} %param.20), kind=kOutput, calls=%fused_computation.29 | convolution fusion | flops 1479901184 | bytes 8594432 | tf_op jit(solution)/shard_map/dot_general | solution.py:142
  172.8 1.3 collective-permute-start
  174.1 1.5 collective-permute-start.1
  175.6 0.0 copy-done.5
  175.6 0.1 slice_reduce_fusion.2
  175.6 0.0 collective-permute-done
  175.6 4.0 collective-permute-done.1
  179.6 1.3 maximum_convert_fusion
  180.9 93.1 %all-gather.6.cloned.1.call-done = bf16[2048,1408]{1,0:T(8,128)(2,1)} async-done(((bf16[512,1408]{1,0:T(8,128)(2,1)}), bf16[2048,1408]{1,0:T(8,128)(2,1)}) %all-gather.6.cloned.1.call-update) | async-done | bytes 5767184 | tf_op jit(solution)/shard_map/all_gather | solution.py:149
  274.0 106.2 %all-gather.8.cloned.1.call-done = bf16[1408,2048]{1,0:T(8,128)(2,1)} async-done(((bf16[1408,512]{1,0:T(8,128)(2,1)}), bf16[1408,2048]{1,0:T(8,128)(2,1)}) %all-gather.8.cloned.1.call-update) | async-done | bytes 5767184 | tf_op jit(solution)/shard_map/all_gather | solution.py:157
  380.2 11.1 %convolution_convert_fusion.3 = bf16[256,2048]{1,0:T(8,128)(2,1)} fusion(bf16[1408,2048]{1,0:T(8,128)(2,1)} %all-gather.8.cloned.1.call-done, bf16[2048,1408]{1,0:T(8,128)(2,1)} %all-gather.6.cloned.1.call-done, f32[258,1408]{1,0:T(8,128)} %maximum_convert_fusion, f32[1408]{0:T(1024)S(1)} %get-tuple-element.91, f32[1408]{0:T(1024)S(1)} %get-tuple-element.92, ...), kind=kOutput, calls=%fused_computation.30 | convolution fusion | flops 2961145856 | bytes 19031552 | tf_op jit(solution)/shard_map/dot_general | solution.py:159
  391.3 0.0 reduce-scatter.2.cloned.1.call-update
  391.3 23.2 %reduce-scatter.2.cloned.1.call-done = bf16[64,2048]{1,0:T(8,128)(2,1)} async-done(((bf16[256,2048]{1,0:T(8,128)(2,1)}), bf16[64,2048]{1,0:T(8,128)(2,1)}) %reduce-scatter.2.cloned.1.call-update) | async-done | bytes 262160 | tf_op jit(solution)/shard_map/reduce_scatter | solution.py:158
  414.5 1.9 add_convert_fusion
  (20 shorter events, 0.2 us)
Async XLA Ops:
  7.4 48.9 %copy-start = (bf16[512,2048]{1,0:T(8,128)(2,1)S(1)}, bf16[512,2048]{1,0:T(8,128)(2,1)}, u32[]{:S(2)}) copy-start(bf16[512,2048]{1,0:T(8,128)(2,1)} %param.19) | copy-start | bytes 6291460
  7.4 5.7 %copy-start.7 = (f32[128]{0:T(128)S(1)}, f32[128]{0:T(128)}, u32[]{:S(2)}) copy-start(f32[128]{0:T(128)} %param.17) | copy-start | bytes 1540
  7.4 88.3 %all-reduce.2.cloned.1.call-start = ((), (), s32[]{:S(2)}) async-start(), calls=%async_computation.1 | async-start | bytes 2097152 | tf_op jit(solution)/shard_map/psum | solution.py:136
  13.4 1.1 copy-start.3
  13.4 1.1 copy-start.6
  13.4 1.7 copy-start.2
  15.1 16.9 %copy-start.4 = (bf16[256,128]{1,0:T(8,128)(2,1)S(1)}, bf16[256,128]{1,0:T(8,128)(2,1)}, u32[]{:S(2)}) copy-start(bf16[256,128]{1,0:T(8,128)(2,1)} %param.16) | copy-start | bytes 196612
  48.4 2.2 copy-start.1
  53.0 2.2 copy-start.1
  58.0 109.6 %all-gather.4.cloned.1.call-start = ((), (), s32[]{:S(2)}) async-start(), calls=%async_computation.2 | async-start | bytes 7208960 | tf_op jit(solution)/shard_map/all_gather | solution.py:144
  58.6 215.4 %all-gather.6.cloned.1.call-start = ((), (), s32[]{:S(2)}) async-start(), calls=%async_computation.3 | async-start | bytes 7208960 | tf_op jit(solution)/shard_map/all_gather | solution.py:149
  59.2 321.0 %all-gather.8.cloned.1.call-start = ((), (), s32[]{:S(2)}) async-start(), calls=%async_computation.4 | async-start | bytes 7208960 | tf_op jit(solution)/shard_map/all_gather | solution.py:157
  59.8 107.8 %copy-start.8 = (f32[2048]{0:T(1024)S(1)}, f32[2048]{0:T(1024)}, u32[]{:S(2)}) copy-start(f32[2048]{0:T(1024)} %param.21) | copy-start | bytes 24580
  59.8 354.7 %reduce-scatter.2.cloned.1.call-start = ((), (), s32[]{:S(2)}) async-start(), calls=%async_computation.5 | async-start | bytes 1310720 | tf_op jit(solution)/shard_map/reduce_scatter | solution.py:158
  98.9 76.6 %copy-start.5 = (f32[3,1408]{1,0:T(4,128)S(1)}, f32[3,1408]{1,0:T(4,128)}, u32[]{:S(2)}) copy-start(f32[3,1408]{1,0:T(4,128)} %param.24) | copy-start | bytes 50692
  172.8 2.8 collective-permute-start
  174.1 5.5 %collective-permute-start.1 = (bf16[1,1408]{1,0:T(2,128)(2,1)S(1)}, bf16[1,1408]{1,0:T(2,128)(2,1)S(1)}, u32[]{:S(2)}, u32[]{:S(2)}) collective-permute-start(bf16[1,1408]{1,0:T(2,128)(2,1)S(1)} %get-tuple-element.117), channel_id=1, source_target_pairs={{4,0},{8,4},{12,8},{5,1},{9,5},{13,9},{6,2},{10,6},{14,10},{7,3},{... | collective-permute-start | bytes 8456 | tf_op jit(solution)/shard_map/ppermute | solution.py:23
Sparse Core Ops, SparseCore 0:
  58.1 37.4 all-reduce.1
  391.4 23.0 reduce-scatter.1
Sparse Core Ops, SparseCore 1:
  60.1 107.5 all-gather.3
  169.0 104.9 all-gather.5
  275.4 104.7 all-gather.7
where the time goes:
time: 424 us
  waiting for transfers between devices  333 us (79%)
  blocking collectives  30.2 us (7%)
  matrix products  22.8 us (5%)
  other arithmetic  16.5 us (4%)
  between operations  15.3 us (4%)
    all_gather x1, waiting for transfers between devices, local(): down_full = lax.all_gather(down_weight, 'sp', axis=1, tiled=True)  106 us
    all_gather x1, waiting for transfers between devices, local(): lax.all_gather(up_weight, 'sp', axis=0, tiled=True)  93.1 us
    all_gather x1, waiting for transfers between devices, local(): lax.all_gather(gate_weight, 'sp', axis=0, tiled=True)  68.7 us
    psum x1, waiting for transfers between devices, local(): lax.psum(jnp.dot(heads, out_weight, preferred_element_type=jnp.float32).a...  35.8 us
    reduce_scatter x1, waiting for transfers between devices, local(): lax.psum_scatter(jnp.dot(hidden, down_full, preferred_element_type=jnp.fl...  23.2 us
    all_gather x1, blocking collectives, local(): key_piece = lax.all_gather(key_flat, 'sp', axis=0, tiled=True)  15.7 us
    all_gather x1, blocking collectives, local(): value_piece = lax.all_gather(values, 'sp', axis=0, tiled=True)  14.6 us
    dot_general x1, matrix products, local(): jnp.dot(hidden, down_full, preferred_element_type=jnp.float32)  11.1 us
  transfers between devices with their start and end apart: 7, of which 6 were waited for; matrix products, arithmetic and copies ran while one was open for 2% of the time, Pallas kernels for 0%

commit v1 on v0

--- a/solution.py
+++ b/solution.py
@@ -1,8 +1,11 @@
+import functools
 import math
 
 import jax
 import jax.numpy as jnp
 from jax import lax
+from jax.experimental import pallas as pl
+from jax.experimental.pallas import tpu as pltpu
 from jax.sharding import PartitionSpec as P
 
 GRID = 64
@@ -164,6 +167,323 @@
     return (mixed_keep + mixer_out).astype(jnp.bfloat16)
 
 
+MESH_ID = pl.DeviceIdType.MESH
+LANES = 128
+
+
+def fused_kernel(
+    n, width, q_ref, k_ref, v_ref, qg_ref, kg_ref, cos_ref, sa_ref, sb_ref, mg_ref, taps_ref,
+    ow_hbm, res_hbm, gw_hbm, uw_hbm, dw_hbm, out_ref,
+    kv, heads, ow, res, pbuf, rc, xs, rx, mixed, ng, wg, wu, wd, gate, up, ps, prc, pxs, prx,
+    pzs, pzr, lsem, kv_s, kv_r, w_s, w_r, y_s, y_r, a_s, a_r, z_s, z_r, x_s, x_r, c_s, c_r,
+    pc_s, pc_r, px_s, px_r, pz_s, pz_r,
+):
+    f32, bf16 = jnp.float32, jnp.bfloat16
+    s = lax.axis_index("sp")
+    t = lax.axis_index("tp")
+    g = lax.axis_index("grp")
+    c = lax.rem(t, 2)
+    x = t // 2
+    core_id = {"tp": 2 * x + 1 - c}
+    x_id = {"tp": lax.rem(t + 2, 4)}
+    y_id = {"grp": 1 - g}
+    rows, hd = k_ref.shape
+    hq = q_ref.shape[1] // hd
+    depth = gw_hbm.shape[0]
+    half = depth // 2
+    hidden_here = gw_hbm.shape[1]
+    part = rows // 4
+    sends = []
+
+    def sp_of(d):
+        return lax.rem(s + d, n)
+
+    def col_start(j):
+        return pl.multiple_of(j * width - (j // (n - 1)) * (n * width - hidden_here), LANES)
+
+    def send(src, dst, ssem, rsem, dev):
+        copy = pltpu.make_async_remote_copy(
+            src_ref=src, dst_ref=dst, send_sem=ssem, recv_sem=rsem, device_id=dev,
+            device_id_type=MESH_ID,
+        )
+        copy.start()
+        sends.append(copy)
+        return copy
+
+    barrier = pltpu.get_barrier_semaphore()
+    peers = [{"sp": sp_of(d)} for d in range(1, n)] + [core_id, x_id, y_id]
+    for dev in peers:
+        pl.semaphore_signal(barrier, inc=1, device_id=dev, device_id_type=MESH_ID)
+
+    mine = col_start(s)
+    block = pl.ds(pl.multiple_of(s * depth, depth), depth)
+    local = [
+        pltpu.make_async_copy(ow_hbm, ow, lsem.at[0]),
+        pltpu.make_async_copy(
+            res_hbm.at[pl.ds(pl.multiple_of(t * part, part), part)], res, lsem.at[1]
+        ),
+        pltpu.make_async_copy(gw_hbm.at[:, pl.ds(mine, width)], wg.at[block], lsem.at[2]),
+        pltpu.make_async_copy(uw_hbm.at[:, pl.ds(mine, width)], wu.at[block], lsem.at[3]),
+        pltpu.make_async_copy(dw_hbm.at[pl.ds(mine, width)], wd.at[s], lsem.at[4]),
+    ]
+    for copy in local:
+        copy.start()
+
+    cos, sa, sb = cos_ref[...], sa_ref[...], sb_ref[...]
+
+    def rotated(field, gain):
+        y = field.astype(f32)
+        y = y * lax.rsqrt(jnp.mean(y * y, axis=-1, keepdims=True) + norm_eps) * gain
+        return (
+            y * cos + pltpu.roll(y, hd // 4, 1) * sa + pltpu.roll(y, hd - hd // 4, 1) * sb
+        ).astype(bf16)
+
+    kv[s, :, :hd] = rotated(k_ref[...], kg_ref[...])
+    kv[s, :, hd:] = v_ref[...]
+    pl.semaphore_wait(barrier, len(peers))
+    kv_copies = [
+        send(kv.at[s], kv.at[s], kv_s.at[d], kv_r.at[d], {"sp": sp_of(d)}) for d in range(1, n)
+    ]
+
+    def wrows(base):
+        return pl.ds(pl.multiple_of(base * depth + g * half, half), half)
+
+    whalf = pl.ds(pl.multiple_of(g * half, half), half)
+    hw = width // 2
+    dhalf = pl.ds(pl.multiple_of(g * hw, hw), hw)
+    w_copies = []
+    for d in range(1, n):
+        j = sp_of(d)
+        for i, (hbm, dst) in enumerate(((gw_hbm, wg), (uw_hbm, wu))):
+            w_copies.append(
+                send(hbm.at[whalf, pl.ds(col_start(j), width)], dst.at[wrows(s)],
+                     w_s.at[i, d], w_r.at[i, d], {"sp": j})
+            )
+
+    def query(h):
+        return rotated(q_ref[:, h * hd : (h + 1) * hd], qg_ref[...])
+
+    queries = [query(h) for h in range(hq)]
+    for copy in kv_copies:
+        copy.wait_recv()
+    key_all = kv[:, :, :hd].reshape(n * rows, hd)
+    value_all = kv[:, :, hd:].reshape(n * rows, hd)
+    scale = hd ** (-0.5)
+    for h in range(hq):
+        scores = lax.dot_general(
+            queries[h], key_all, (((1,), (1,)), ((), ())), preferred_element_type=f32
+        ) * scale
+        expo = jnp.exp(scores - jnp.max(scores, axis=-1, keepdims=True))
+        totals = jnp.sum(expo, axis=-1, keepdims=True)
+        mix = jnp.dot(expo.astype(bf16), value_all, preferred_element_type=f32) / totals
+        heads[:, h * hd : (h + 1) * hd] = mix.astype(bf16)
+    local[0].wait()
+    dim = ow.shape[1]
+    pbuf[...] = (
+        jnp.dot(heads[...], ow[...], preferred_element_type=f32).astype(bf16)
+        .reshape(4, part, dim)
+    )
+    a_copies = [
+        send(pbuf.at[2 * e + 1 - c], rc.at[e], a_s.at[e], a_r.at[e], core_id) for e in range(2)
+    ]
+    for copy in a_copies:
+        copy.wait_recv()
+    xs[...] = (
+        pbuf[2 * (1 - x) + c].astype(f32) + rc[1 - x].astype(f32)
+    ).astype(bf16)
+    ax = send(xs, rx, a_s.at[2], a_r.at[2], x_id)
+    local[1].wait()
+    ax.wait_recv()
+    total = pbuf[t].astype(f32) + rc[x].astype(f32) + rx[...].astype(f32)
+    total = total + res[...].astype(f32)
+    mixed[...] = total
+    ng[s, t] = (
+        total * lax.rsqrt(jnp.mean(total * total, axis=-1, keepdims=True) + norm_eps)
+        * mg_ref[...]
+    ).astype(bf16)
+
+    own = ng.at[s, t]
+    z_copies = [None] + [
+        send(own, own, z_s.at[d], z_r.at[d], {"sp": sp_of(d)}) for d in range(1, n)
+    ]
+    x_copies, c_copies = [], []
+
+    def relay(d):
+        piece = ng.at[sp_of(n - d), t]
+        x_copies.append(send(piece, piece, x_s.at[d], x_r.at[d], x_id))
+        c_copies.append(send(piece, piece, c_s.at[0, d], c_r.at[0, d], core_id))
+
+    relay(0)
+    d_copies = []
+    for d in range(1, n):
+        j = sp_of(d)
+        rows_j = pl.ds(pl.multiple_of(col_start(j) + g * hw, LANES // 2), hw)
+        d_copies.append(
+            send(dw_hbm.at[rows_j], wd.at[s, dhalf], w_s.at[2, d], w_r.at[2, d], {"sp": j})
+        )
+    y_copies = []
+    k = 0
+    for d in range(1, n):
+        for i, dst in enumerate((wg, wu)):
+            w_copies[k].wait_recv()
+            k += 1
+            piece = dst.at[wrows(sp_of(n - d))]
+            y_copies.append(send(piece, piece, y_s.at[i, d], y_r.at[i, d], y_id))
+
+    gate[0:8] = jnp.zeros((8, width), f32)
+    gate[n * rows + 8 : n * rows + 16] = jnp.zeros((8, width), f32)
+    for d in range(n):
+        if d + 1 < n:
+            z_copies[d + 1].wait_recv()
+            relay(d + 1)
+        x_copies[d].wait_recv()
+        src = sp_of(n - d)
+        piece = ng.at[src, lax.rem(t + 2, 4)]
+        fwd = send(piece, piece, c_s.at[1, d], c_r.at[1, d], core_id)
+        if d == 0:
+            local[2].wait()
+            local[3].wait()
+            for copy in y_copies:
+                copy.wait_recv()
+        c_copies[d].wait_recv()
+        fwd.wait_recv()
+        tokens = ng[src].reshape(rows, dim)
+        at = pl.ds(pl.multiple_of(src * rows + 8, 8), rows)
+        gate[at] = jnp.dot(tokens, wg[...], preferred_element_type=f32).astype(bf16).astype(f32)
+        up[src] = jnp.dot(tokens, wu[...], preferred_element_type=f32).astype(bf16)
+    yd_copies = []
+    for d in range(1, n):
+        d_copies[d - 1].wait_recv()
+        piece = wd.at[sp_of(n - d), dhalf]
+        yd_copies.append(send(piece, piece, y_s.at[2, d], y_r.at[2, d], y_id))
+    column = mine + lax.broadcasted_iota(jnp.int32, (rows, width), 1)
+    keep = column >= s * width
+
+    def stage_hidden(i):
+        dst = sp_of(1 + i)
+        window = gate[pl.ds(pl.multiple_of(dst * rows, 8), rows + 16)]
+        taps = taps_ref[...]
+        conv = (
+            taps[0:1] * window[7 : 7 + rows]
+            + taps[1:2] * window[8 : 8 + rows]
+            + taps[2:3] * window[9 : 9 + rows]
+        )
+        hid = jax.nn.silu(conv) * up[dst].astype(f32)
+        return jnp.where(keep, hid, 0.0).astype(bf16)
+
+    pcs, pxc, pzc = {}, {}, {}
+
+    def stage_a(i):
+        hid = stage_hidden(i)
+        if i == 0:
+            local[4].wait()
+            for copy in yd_copies:
+                copy.wait_recv()
+        for b in range(n):
+            ps[i, :, :, b * depth : (b + 1) * depth] = (
+                jnp.dot(hid, wd[b], preferred_element_type=f32).astype(bf16)
+                .reshape(4, part, depth)
+            )
+        pcs[i] = [
+            send(ps.at[i, 2 * e + 1 - c], prc.at[i, e], pc_s.at[i, e], pc_r.at[i, e], core_id)
+            for e in range(2)
+        ]
+
+    def stage_b(i):
+        for copy in pcs[i]:
+            copy.wait_recv()
+        pxs[i] = (
+            ps[i, 2 * (1 - x) + c].astype(f32) + prc[i, 1 - x].astype(f32)
+        ).astype(bf16)
+        pxc[i] = send(pxs.at[i], prx.at[i], px_s.at[i], px_r.at[i], x_id)
+
+    def stage_c(i):
+        pxc[i].wait_recv()
+        total = ps[i, t].astype(f32) + prc[i, x].astype(f32) + prx[i].astype(f32)
+        if i == n - 1:
+            mixed[...] += total
+        else:
+            pzs[i] = total.astype(bf16)
+            pzc[i] = send(pzs.at[i], pzr.at[i], pz_s.at[i], pz_r.at[i], {"sp": sp_of(1 + i)})
+
+    for i in range(n + 2):
+        if i < n:
+            stage_a(i)
+        if 0 <= i - 1 < n:
+            stage_b(i - 1)
+        if 0 <= i - 2 < n:
+            stage_c(i - 2)
+    final = mixed[...]
+    for i in range(n - 1):
+        pzc[i].wait_recv()
+        final = final + pzr[i].astype(f32)
+    out_ref[...] = final.astype(bf16)
+    for copy in sends:
+        copy.wait_send()
+
+
+def fused(n, width, queries, keys, values, query_gain, key_norm_gain, out_weight, residual,
+          mixer_gain, gate_weight, up_weight, conv_taps, down_weight):
+    rows, hd = keys.shape
+    dim = residual.shape[1]
+    part = rows // 4
+    bf16, f32 = jnp.bfloat16, jnp.float32
+    s = lax.axis_index("sp")
+    positions = s * rows + jnp.arange(rows, dtype=jnp.int32)
+    cos, sin = angle_tables(positions, hd)
+    odd = (jnp.arange(hd) // (hd // 4)) % 2 == 1
+    sa = jnp.where(odd, sin, 0.0)
+    sb = jnp.where(odd, 0.0, -sin)
+    start = jnp.minimum(s * width, conv_taps.shape[1] - width)
+    taps = lax.dynamic_slice_in_dim(conv_taps, start, width, 1)
+    vm = pl.BlockSpec(memory_space=pltpu.VMEM)
+    hbm = pl.BlockSpec(memory_space=pl.ANY)
+    dma = pltpu.SemaphoreType.DMA
+    V = pltpu.VMEM
+    scratch = [
+        V((n, rows, 2 * hd), bf16), V((rows, queries.shape[1]), bf16),
+        V(out_weight.shape, bf16), V((part, dim), bf16), V((4, part, dim), bf16),
+        V((2, part, dim), bf16), V((part, dim), bf16), V((part, dim), bf16), V((part, dim), f32),
+        V((n, 4, part, dim), bf16), V((dim, width), bf16), V((dim, width), bf16),
+        V((n, width, dim // n), bf16), V((n * rows + 16, width), f32), V((n, rows, width), bf16),
+        V((n, 4, part, dim), bf16), V((n, 2, part, dim), bf16), V((n, part, dim), bf16),
+        V((n, part, dim), bf16), V((n - 1, part, dim), bf16), V((n - 1, part, dim), bf16),
+        dma((5,)), dma((n,)), dma((n,)), dma((3, n)), dma((3, n)), dma((3, n)), dma((3, n)),
+        dma((3,)), dma((3,)), dma((n,)), dma((n,)), dma((n,)), dma((n,)), dma((2, n)),
+        dma((2, n)), dma((n, 2)), dma((n, 2)), dma((n,)), dma((n,)), dma((n,)), dma((n,)),
+    ]
+    return pl.pallas_call(
+        functools.partial(fused_kernel, n, width),
+        out_shape=jax.ShapeDtypeStruct((part, dim), bf16),
+        in_specs=[vm] * 10 + [hbm] * 5,
+        out_specs=vm,
+        scratch_shapes=scratch,
+        compiler_params=pltpu.CompilerParams(
+            collective_id=0, has_side_effects=True, vmem_limit_bytes=60 * 1024 * 1024
+        ),
+    )(queries, keys, values, query_gain[None], key_norm_gain[None], cos, sa, sb,
+      mixer_gain[None], taps, out_weight, residual, gate_weight, up_weight, down_weight)
+
+
+def block_width(n, hidden_here):
+    return -(-hidden_here // (n * LANES)) * LANES
+
+
+def dispatch(*args):
+    queries, keys, gate_weight = args[0], args[1], args[8]
+    n = lax.axis_size("sp")
+    hidden_here = gate_weight.shape[1]
+    width = block_width(n, hidden_here)
+    fits = (n - 1) * width < hidden_here and n * keys.shape[0] <= 2048
+    if (
+        n > 1 and fits and lax.axis_size("tp") == 4 and lax.axis_size("grp") == 2
+        and keys.shape[1] == args[3].shape[0] and keys.shape[0] % 64 == 0
+        and hidden_here % LANES == 0
+    ):
+        return fused(n, width, *args)
+    return local(*args)
+
+
 def solution(mesh):
     in_specs = (
         P(("grp", "sp"), "tp"),
@@ -180,4 +500,4 @@
         P("tp", "sp"),
     )
     out_specs = P(("grp", "sp", "tp"), None)
-    return jax.shard_map(local, mesh=mesh, in_specs=in_specs, out_specs=out_specs, check_vma=False)
+    return jax.shard_map(dispatch, mesh=mesh, in_specs=in_specs, out_specs=out_specs, check_vma=False)

time: 424 us -> 153 us (0.36)
  the two profiles are of different devices: /device:TPU:0 before, /device:TPU:9 now
where the time goes in v1:
time: 153 us; the launch traced here: 152 us
  Pallas kernels  149 us (97%)
  local copies, waits for them, and re-layouts  2.34 us (2%)
    pallas_call x1, Pallas kernels, fused(): pl.pallas_call(functools.partial(fused_kernel, n, width), out_shape=jax.S...  149 us

profile of v1, /device:TPU:9, one launch (start us, length us, event | category | flops | bytes accessed | tf_op | source)
XLA Modules:
  0.0 152.4 jit_solution(13460786006146521298)
XLA Ops:
  0.0 0.0 copy-start
  0.0 0.1 broadcast_multiply_fusion.1
  0.2 1.3 negate_select_fusion
  1.5 0.0 copy-done
  1.5 0.7 constant_dynamic-slice_fusion.taps_ref
  2.2 148.6 %shard_map.118 = bf16[64,2048]{1,0:T(8,128)(2,1)} custom-call(bf16[256,512]{1,0:T(8,128)(2,1)} %q_ref.1, bf16[256,128]{1,0:T(8,128)(2,1)} %k_ref.1, bf16[256,128]{1,0:T(8,128)(2,1)} %v_ref.1, f32[1,128]{1,0:T(1,128)} %bitcast.4, f32[1,128]{1,0:T(1,128)} %bitcast.5, f32[256,128]{1,0:T(8,128)} %get-tuple-element.7.cos_ref, ...), custom_call_target="tpu_custom_call" | custom-call | tf_op jit(solution)/shard_map/pallas_call | solution.py:455
  150.8 1.7 %copy.14 = bf16[64,2048]{1,0:T(8,128)(2,1)} copy(bf16[64,2048]{1,0:T(8,128)(2,1)} %shard_map.118) | data formatting | bytes 524288
  (3 shorter events, 0.0 us)
Async XLA Ops:
  0.0 1.5 copy-start

commit v2 on v1

--- a/solution.py
+++ b/solution.py
@@ -172,9 +172,9 @@
 
 
 def fused_kernel(
-    n, width, q_ref, k_ref, v_ref, qg_ref, kg_ref, cos_ref, sa_ref, sb_ref, mg_ref, taps_ref,
-    ow_hbm, res_hbm, gw_hbm, uw_hbm, dw_hbm, out_ref,
-    kv, heads, ow, res, pbuf, rc, xs, rx, mixed, ng, wg, wu, wd, gate, up, ps, prc, pxs, prx,
+    n, width, q_ref, k_ref, v_ref, qg_ref, kg_ref, cos_ref, sa_ref, sb_ref, mg_ref,
+    ow_hbm, res_hbm, gw_hbm, uw_hbm, dw_hbm, taps_hbm, out_ref,
+    kv, heads, ow, res, pbuf, rc, xs, rx, mixed, ng, wg, wu, wd, taps_ref, gate, up, hid, ps, prc, pxs, prx,
     pzs, pzr, lsem, kv_s, kv_r, w_s, w_r, y_s, y_r, a_s, a_r, z_s, z_r, x_s, x_r, c_s, c_r,
     pc_s, pc_r, px_s, px_r, pz_s, pz_r,
 ):
@@ -193,6 +193,7 @@
     half = depth // 2
     hidden_here = gw_hbm.shape[1]
     part = rows // 4
+    cols = dw_hbm.shape[1]
     sends = []
 
     def sp_of(d):
@@ -225,6 +226,7 @@
         pltpu.make_async_copy(gw_hbm.at[:, pl.ds(mine, width)], wg.at[block], lsem.at[2]),
         pltpu.make_async_copy(uw_hbm.at[:, pl.ds(mine, width)], wu.at[block], lsem.at[3]),
         pltpu.make_async_copy(dw_hbm.at[pl.ds(mine, width)], wd.at[s], lsem.at[4]),
+        pltpu.make_async_copy(taps_hbm.at[:, pl.ds(mine, width)], taps_ref, lsem.at[5]),
     ]
     for copy in local:
         copy.start()
@@ -315,12 +317,6 @@
 
     relay(0)
     d_copies = []
-    for d in range(1, n):
-        j = sp_of(d)
-        rows_j = pl.ds(pl.multiple_of(col_start(j) + g * hw, LANES // 2), hw)
-        d_copies.append(
-            send(dw_hbm.at[rows_j], wd.at[s, dhalf], w_s.at[2, d], w_r.at[2, d], {"sp": j})
-        )
     y_copies = []
     k = 0
     for d in range(1, n):
@@ -332,60 +328,86 @@
 
     gate[0:8] = jnp.zeros((8, width), f32)
     gate[n * rows + 8 : n * rows + 16] = jnp.zeros((8, width), f32)
-    for d in range(n):
-        if d + 1 < n:
-            z_copies[d + 1].wait_recv()
-            relay(d + 1)
+    forwards = []
+
+    def pass_on(d):
         x_copies[d].wait_recv()
-        src = sp_of(n - d)
-        piece = ng.at[src, lax.rem(t + 2, 4)]
-        fwd = send(piece, piece, c_s.at[1, d], c_r.at[1, d], core_id)
+        piece = ng.at[sp_of(n - d), lax.rem(t + 2, 4)]
+        forwards.append(send(piece, piece, c_s.at[1, d], c_r.at[1, d], core_id))
+
+    def take_next(d):
+        z_copies[d].wait_recv()
+        relay(d)
+
+    def send_down():
+        for d in range(1, n):
+            j = sp_of(d)
+            rows_j = pl.ds(pl.multiple_of(col_start(j) + g * hw, LANES // 2), hw)
+            d_copies.append(
+                send(dw_hbm.at[rows_j], wd.at[s, dhalf], w_s.at[2, d], w_r.at[2, d], {"sp": j})
+            )
+
+    def project(d):
         if d == 0:
             local[2].wait()
             local[3].wait()
             for copy in y_copies:
                 copy.wait_recv()
         c_copies[d].wait_recv()
-        fwd.wait_recv()
+        forwards[d].wait_recv()
+        src = sp_of(n - d)
         tokens = ng[src].reshape(rows, dim)
         at = pl.ds(pl.multiple_of(src * rows + 8, 8), rows)
         gate[at] = jnp.dot(tokens, wg[...], preferred_element_type=f32).astype(bf16).astype(f32)
         up[src] = jnp.dot(tokens, wu[...], preferred_element_type=f32).astype(bf16)
-    yd_copies = []
+
     for d in range(1, n):
+        take_next(d)
+        if d == n - 1:
+            send_down()
+        pass_on(d - 1)
+        if d >= 2:
+            project(d - 2)
+    if n > 1:
+        project(n - 2)
+    pass_on(n - 1)
+    project(n - 1)
+
+    yd_copies = {}
+
+    def forward_down(d):
         d_copies[d - 1].wait_recv()
         piece = wd.at[sp_of(n - d), dhalf]
-        yd_copies.append(send(piece, piece, y_s.at[2, d], y_r.at[2, d], y_id))
+        yd_copies[d] = send(piece, piece, y_s.at[2, d], y_r.at[2, d], y_id)
+
+    forward_down(1)
     column = mine + lax.broadcasted_iota(jnp.int32, (rows, width), 1)
     keep = column >= s * width
-
-    def stage_hidden(i):
-        dst = sp_of(1 + i)
-        window = gate[pl.ds(pl.multiple_of(dst * rows, 8), rows + 16)]
-        taps = taps_ref[...]
+    local[5].wait()
+    taps = taps_ref[...]
+    for r in range(n):
+        window = gate[r * rows : (r + 1) * rows + 16]
         conv = (
             taps[0:1] * window[7 : 7 + rows]
             + taps[1:2] * window[8 : 8 + rows]
             + taps[2:3] * window[9 : 9 + rows]
         )
-        hid = jax.nn.silu(conv) * up[dst].astype(f32)
-        return jnp.where(keep, hid, 0.0).astype(bf16)
+        act = jax.nn.silu(conv) * up[r].astype(f32)
+        hid[r * rows : (r + 1) * rows] = jnp.where(keep, act, 0.0).astype(bf16)
 
     pcs, pxc, pzc = {}, {}, {}
 
     def stage_a(i):
-        hid = stage_hidden(i)
         if i == 0:
             local[4].wait()
-            for copy in yd_copies:
-                copy.wait_recv()
-        for b in range(n):
-            ps[i, :, :, b * depth : (b + 1) * depth] = (
-                jnp.dot(hid, wd[b], preferred_element_type=f32).astype(bf16)
-                .reshape(4, part, depth)
-            )
+        else:
+            yd_copies[i].wait_recv()
+        ps[i] = (
+            jnp.dot(hid[...], wd[sp_of(n - i)], preferred_element_type=f32).astype(bf16)
+            .reshape(n, 4, part, cols)
+        )
         pcs[i] = [
-            send(ps.at[i, 2 * e + 1 - c], prc.at[i, e], pc_s.at[i, e], pc_r.at[i, e], core_id)
+            send(ps.at[i, :, 2 * e + 1 - c], prc.at[i, e], pc_s.at[i, e], pc_r.at[i, e], core_id)
             for e in range(2)
         ]
 
@@ -393,31 +415,41 @@
         for copy in pcs[i]:
             copy.wait_recv()
         pxs[i] = (
-            ps[i, 2 * (1 - x) + c].astype(f32) + prc[i, 1 - x].astype(f32)
+            ps[i, :, 2 * (1 - x) + c].astype(f32) + prc[i, 1 - x].astype(f32)
         ).astype(bf16)
         pxc[i] = send(pxs.at[i], prx.at[i], px_s.at[i], px_r.at[i], x_id)
 
+    def columns_of(owner):
+        return pl.ds(pl.multiple_of(owner * cols, LANES), cols)
+
     def stage_c(i):
         pxc[i].wait_recv()
-        total = ps[i, t].astype(f32) + prc[i, x].astype(f32) + prx[i].astype(f32)
-        if i == n - 1:
-            mixed[...] += total
-        else:
-            pzs[i] = total.astype(bf16)
-            pzc[i] = send(pzs.at[i], pzr.at[i], pz_s.at[i], pz_r.at[i], {"sp": sp_of(1 + i)})
+        pzs[i] = (
+            ps[i, :, t].astype(f32) + prc[i, x].astype(f32) + prx[i].astype(f32)
+        ).astype(bf16)
+        for d in range(1, n):
+            j = sp_of(d)
+            pzc[i, d] = send(
+                pzs.at[i, j], pzr.at[i, d], pz_s.at[i, d], pz_r.at[i, d], {"sp": j}
+            )
+        mixed[:, columns_of(sp_of(n - i))] += (
+            ps[i, s, t].astype(f32) + prc[i, x, s].astype(f32) + prx[i, s].astype(f32)
+        )
 
     for i in range(n + 2):
         if i < n:
             stage_a(i)
         if 0 <= i - 1 < n:
             stage_b(i - 1)
+        if i + 2 < n:
+            forward_down(i + 2)
         if 0 <= i - 2 < n:
             stage_c(i - 2)
-    final = mixed[...]
-    for i in range(n - 1):
-        pzc[i].wait_recv()
-        final = final + pzr[i].astype(f32)
-    out_ref[...] = final.astype(bf16)
+    for i in range(n):
+        for d in range(1, n):
+            pzc[i, d].wait_recv()
+            mixed[:, columns_of(sp_of(2 * n - d - i))] += pzr[i, d].astype(f32)
+    out_ref[...] = mixed[...].astype(bf16)
     for copy in sends:
         copy.wait_send()
 
@@ -426,6 +458,7 @@
           mixer_gain, gate_weight, up_weight, conv_taps, down_weight):
     rows, hd = keys.shape
     dim = residual.shape[1]
+    cols = down_weight.shape[1]
     part = rows // 4
     bf16, f32 = jnp.bfloat16, jnp.float32
     s = lax.axis_index("sp")
@@ -434,8 +467,6 @@
     odd = (jnp.arange(hd) // (hd // 4)) % 2 == 1
     sa = jnp.where(odd, sin, 0.0)
     sb = jnp.where(odd, 0.0, -sin)
-    start = jnp.minimum(s * width, conv_taps.shape[1] - width)
-    taps = lax.dynamic_slice_in_dim(conv_taps, start, width, 1)
     vm = pl.BlockSpec(memory_space=pltpu.VMEM)
     hbm = pl.BlockSpec(memory_space=pl.ANY)
     dma = pltpu.SemaphoreType.DMA
@@ -445,24 +476,25 @@
         V(out_weight.shape, bf16), V((part, dim), bf16), V((4, part, dim), bf16),
         V((2, part, dim), bf16), V((part, dim), bf16), V((part, dim), bf16), V((part, dim), f32),
         V((n, 4, part, dim), bf16), V((dim, width), bf16), V((dim, width), bf16),
-        V((n, width, dim // n), bf16), V((n * rows + 16, width), f32), V((n, rows, width), bf16),
-        V((n, 4, part, dim), bf16), V((n, 2, part, dim), bf16), V((n, part, dim), bf16),
-        V((n, part, dim), bf16), V((n - 1, part, dim), bf16), V((n - 1, part, dim), bf16),
-        dma((5,)), dma((n,)), dma((n,)), dma((3, n)), dma((3, n)), dma((3, n)), dma((3, n)),
+        V((n, width, cols), bf16), V((conv_taps.shape[0], width), f32),
+        V((n * rows + 16, width), f32), V((n, rows, width), bf16), V((n * rows, width), bf16),
+        V((n, n, 4, part, cols), bf16), V((n, 2, n, part, cols), bf16), V((n, n, part, cols), bf16),
+        V((n, n, part, cols), bf16), V((n, n, part, cols), bf16), V((n, n, part, cols), bf16),
+        dma((6,)), dma((n,)), dma((n,)), dma((3, n)), dma((3, n)), dma((3, n)), dma((3, n)),
         dma((3,)), dma((3,)), dma((n,)), dma((n,)), dma((n,)), dma((n,)), dma((2, n)),
-        dma((2, n)), dma((n, 2)), dma((n, 2)), dma((n,)), dma((n,)), dma((n,)), dma((n,)),
+        dma((2, n)), dma((n, 2)), dma((n, 2)), dma((n,)), dma((n,)), dma((n, n)), dma((n, n)),
     ]
     return pl.pallas_call(
         functools.partial(fused_kernel, n, width),
         out_shape=jax.ShapeDtypeStruct((part, dim), bf16),
-        in_specs=[vm] * 10 + [hbm] * 5,
+        in_specs=[vm] * 9 + [hbm] * 6,
         out_specs=vm,
         scratch_shapes=scratch,
         compiler_params=pltpu.CompilerParams(
             collective_id=0, has_side_effects=True, vmem_limit_bytes=60 * 1024 * 1024
         ),
     )(queries, keys, values, query_gain[None], key_norm_gain[None], cos, sa, sb,
-      mixer_gain[None], taps, out_weight, residual, gate_weight, up_weight, down_weight)
+      mixer_gain[None], out_weight, residual, gate_weight, up_weight, down_weight, conv_taps)
 
 
 def block_width(n, hidden_here):

time: 153 us -> 133 us (0.87)
  the two profiles are of different devices: /device:TPU:9 before, /device:TPU:0 now
where the time goes in v2:
time: 133 us
  Pallas kernels  130 us (98%)
  local copies, waits for them, and re-layouts  1.67 us (1%)
  other arithmetic  1.48 us (1%)
    pallas_call x1, Pallas kernels, fused(): pl.pallas_call(functools.partial(fused_kernel, n, width), out_shape=jax.S...  130 us

profile of v2, /device:TPU:0, one launch (start us, length us, event | category | flops | bytes accessed | tf_op | source)
XLA Modules:
  0.0 132.9 jit_solution(16531482631376703612)
XLA Ops:
  0.0 0.1 broadcast_multiply_fusion.1
  0.2 1.3 negate_select_fusion
  1.5 129.7 %shard_map.118 = bf16[64,2048]{1,0:T(8,128)(2,1)} custom-call(bf16[256,512]{1,0:T(8,128)(2,1)} %q_ref.1, bf16[256,128]{1,0:T(8,128)(2,1)} %k_ref.1, bf16[256,128]{1,0:T(8,128)(2,1)} %v_ref.1, f32[1,128]{1,0:T(1,128)} %bitcast.4, f32[1,128]{1,0:T(1,128)} %bitcast.5, f32[256,128]{1,0:T(8,128)} %get-tuple-element.7.cos_ref, ...), custom_call_target="tpu_custom_call" | custom-call | tf_op jit(solution)/shard_map/pallas_call | solution.py:487
  131.2 1.7 %copy.14 = bf16[64,2048]{1,0:T(8,128)(2,1)} copy(bf16[64,2048]{1,0:T(8,128)(2,1)} %shard_map.118) | data formatting | bytes 524288
  (3 shorter events, 0.0 us)
